TPU v7x, 32 devices: a whole 2x2x4 slice. The times are simulated.
32 devices in a mesh: rep: 4 (over z), fs: 4 (over y, x), tp: 2 (over core).
Axes of the slice: x: 2, y: 2, z: 4, core: 2. Of those that a mesh axis runs over, the one named last changes fastest.
Arguments:
- tokens_in: bfloat16 [3072, 1024], P(('rep', 'fs', 'tp')), may hold values from -6 to 6
- out_grad: bfloat16 [3072, 1024], P(('rep', 'fs', 'tp')), may hold values from -6 to 6
- gate_weight: bfloat16 [1024, 2816], P('fs', 'tp'), may hold values from -0.1875 to 0.1875
- up_weight: bfloat16 [1024, 2816], P('fs', 'tp'), may hold values from -0.1875 to 0.1875
- down_weight: bfloat16 [2816, 1024], P('tp', 'fs'), may hold values from -0.109375 to 0.109375
Outputs:
- grad_in: bfloat16 [3072, 1024], P(('rep', 'fs', 'tp'))
- grad_gate_w: float32 [1024, 2816], P('fs', 'tp')
- grad_up_w: float32 [1024, 2816], P('fs', 'tp')
- grad_down_w: float32 [2816, 1024], P('tp', 'fs')
All inputs are finite; a program needn't handle non-finite values.
Results may differ from a plain program's by a relative error of at most 0.02.
Values may be sent and summed in bfloat16 or wider, within the bound.
A program may use at most 64 MiB of HBM per device.

v0:
```python
import jax
import jax.numpy as jnp
from jax import lax
from jax.sharding import PartitionSpec as P


def summed_rows(product, width, axis):
    everything = product(jnp.int32(0), lax.axis_size(axis) * width)
    own = lax.psum_scatter(everything.astype(jnp.bfloat16), axis, scatter_dimension=0, tiled=True)
    return own.astype(jnp.float32)


def regroup(block, outer, inner, dimension):
    old_shape = block.shape
    width = old_shape[dimension] // (outer * inner)
    new_shape = old_shape[:dimension] + (outer, inner, width) + old_shape[dimension + 1 :]
    layout = list(range(len(new_shape)))
    layout[dimension] = dimension + 1
    layout[dimension + 1] = dimension
    return jnp.transpose(block.reshape(new_shape), layout).reshape(old_shape)


def contract_last(left, right):
    return lax.dot_general(
        left, right, (((1,), (1,)), ((), ())), preferred_element_type=jnp.float32
    )


def contract_first(left, right):
    return lax.dot_general(
        left, right, (((0,), (0,)), ((), ())), preferred_element_type=jnp.float32
    )


def body(tokens_in, out_grad, gate_weight, up_weight, down_weight):
    replicas = lax.axis_size("rep")
    shards = lax.axis_size("fs")
    columns = lax.axis_size("tp")
    local_rows = tokens_in.shape[0]
    model_width = gate_weight.shape[0] * shards
    hidden_cols = gate_weight.shape[1]
    factor = (local_rows * replicas * shards * columns) ** (-0.5)
    part_rows = gate_weight.shape[0] // replicas
    offset = lax.axis_index("rep") * part_rows
    pieces = (
        lax.dynamic_slice_in_dim(gate_weight, offset, part_rows, 0),
        lax.dynamic_slice_in_dim(up_weight, offset, part_rows, 0),
        lax.dynamic_slice_in_dim(down_weight, offset, part_rows, 1),
    )
    gate_full, up_full, down_full = (
        lax.all_gather(pieces[0], ("rep", "fs"), axis=0, tiled=True),
        lax.all_gather(pieces[1], ("rep", "fs"), axis=0, tiled=True),
        lax.all_gather(pieces[2], ("rep", "fs"), axis=1, tiled=True),
    )
    gate_full = regroup(gate_full, replicas, shards, 0)
    up_full = regroup(up_full, replicas, shards, 0)
    down_full = regroup(down_full, replicas, shards, 1)
    tokens_all, grads_all = (
        lax.all_gather(tokens_in, "tp", axis=0, tiled=True),
        lax.all_gather(out_grad, "tp", axis=0, tiled=True),
    )
    gate = jnp.dot(tokens_all, gate_full, preferred_element_type=jnp.float32).astype(jnp.bfloat16)
    up_proj = jnp.dot(tokens_all, up_full, preferred_element_type=jnp.float32).astype(jnp.bfloat16)
    gate_wide = gate.astype(jnp.float32)
    up_wide = up_proj.astype(jnp.float32)
    sigmoid = jax.nn.sigmoid(gate_wide)
    activated = gate_wide * sigmoid
    hidden = (activated * up_wide).astype(jnp.bfloat16)
    grad_hidden = contract_last(grads_all, down_full).astype(jnp.bfloat16)
    grad_wide = grad_hidden.astype(jnp.float32)
    grad_gate = (grad_wide * up_wide * sigmoid * (1.0 + gate_wide * (1.0 - sigmoid))).astype(
        jnp.bfloat16
    )
    grad_up = (grad_wide * activated).astype(jnp.bfloat16)

    def input_term(start, count):
        gate_rows = lax.dynamic_slice_in_dim(grad_gate, start, count, 0)
        up_rows = lax.dynamic_slice_in_dim(grad_up, start, count, 0)
        return contract_last(gate_rows, gate_full) + contract_last(up_rows, up_full)

    grad_in = summed_rows(input_term, local_rows, "tp").astype(jnp.bfloat16)

    def weight_term(token_order, grad_order):

        def term(start, count):
            token_cols = lax.dynamic_slice_in_dim(token_order, start, count, 1)
            grad_cols = lax.dynamic_slice_in_dim(grad_order, start, count, 1)
            return factor * jnp.concatenate(
                [
                    contract_first(token_cols, grad_gate),
                    contract_first(token_cols, grad_up),
                    contract_first(grad_cols, hidden),
                ],
                axis=1,
            )

        return term

    owned = summed_rows(weight_term(tokens_all, grads_all), model_width // shards, "fs")
    summed = lax.psum(owned.astype(jnp.bfloat16), "rep").astype(jnp.float32)
    grad_gate_w = summed[:, :hidden_cols]
    grad_up_w = summed[:, hidden_cols : 2 * hidden_cols]
    grad_down_w = summed[:, 2 * hidden_cols :].T
    return (grad_in, grad_gate_w, grad_up_w, grad_down_w)


def solution(mesh):
    placed = (
        P(("rep", "fs", "tp"), None),
        P(("rep", "fs", "tp"), None),
        P("fs", "tp"),
        P("fs", "tp"),
        P("tp", "fs"),
    )
    return jax.shard_map(
        body,
        mesh=mesh,
        in_specs=placed,
        out_specs=(P(("rep", "fs", "tp"), None), P("fs", "tp"), P("fs", "tp"), P("tp", "fs")),
        check_vma=False,
    )
```

profile of v0, /device:TPU:0, one launch (start us, length us, event | category | flops | bytes accessed | tf_op | source)
XLA Modules:
  0.0 423.5 jit_solution(640800213981886636)
XLA Ops:
  7.2 0.0 copy-start
  7.2 0.0 copy-start.9
  7.2 0.0 copy-start.10
  7.2 0.0 all-gather.8.cloned.1.call-start
  7.3 1.0 copy-done
  8.3 0.7 constant_dynamic-slice_fusion
  9.0 0.0 all-gather.8.cloned.1.call-update
  9.0 0.0 all-gather.6.cloned.1.call-start
  9.0 1.6 constant_dynamic-slice_fusion.1
  10.7 0.0 all-gather.6.cloned.1.call-update
  10.7 0.0 all-gather.4.cloned.1.call-start
  10.7 1.2 constant_dynamic-slice_fusion.2
  11.9 0.8 copy.21
  12.7 0.0 all-gather.4.cloned.1.call-update
  12.7 0.0 reduce-scatter.5.cloned.1.call-start
  12.8 0.0 copy-done.9
  12.8 2.2 all_gather.18
  15.0 0.0 copy-done.10
  15.0 2.2 all_gather.16
  17.3 63.1 %all-gather.8.cloned.1.call-done = bf16[1024,1408]{1,0:T(8,128)(2,1)} async-done(((bf16[64,1408]{1,0:T(8,128)(2,1)}), bf16[1024,1408]{1,0:T(8,128)(2,1)}) %all-gather.8.cloned.1.call-update) | async-done | bytes 2883600 | tf_op jit(solution)/shard_map/all_gather | solution.py:51
  80.4 2.1 copy.18
  82.5 65.9 %all-gather.6.cloned.1.call-done = bf16[1024,1408]{1,0:T(8,128)(2,1)} async-done(((bf16[64,1408]{1,0:T(8,128)(2,1)}), bf16[1024,1408]{1,0:T(8,128)(2,1)}) %all-gather.6.cloned.1.call-update) | async-done | bytes 2883600 | tf_op jit(solution)/shard_map/all_gather | solution.py:52
  148.4 3.7 copy.17
  152.1 64.4 %all-gather.4.cloned.1.call-done = bf16[1408,1024]{0,1:T(8,128)(2,1)} async-done(((bf16[1408,64]{0,1:T(8,128)(2,1)}), bf16[1408,1024]{0,1:T(8,128)(2,1)}) %all-gather.4.cloned.1.call-update) | async-done | bytes 2883600 | tf_op jit(solution)/shard_map/all_gather | solution.py:53
  216.4 0.0 copy-start.2
  216.5 2.2 copy.16
  218.7 0.5 copy-done.2
  219.1 0.8 fusion.4
  219.9 0.0 copy-start.8
  219.9 0.8 fusion.2
  220.7 0.2 copy-done.8
  220.9 1.0 convolution_bitcast_fusion
  221.9 0.9 multiply_convert_fusion.1
  222.8 0.0 copy-start.5
  222.8 0.0 copy-start.7
  222.8 0.9 convolution_bitcast_fusion.1
  223.8 0.0 copy-done.5
  223.8 0.0 copy-done.7
  223.8 1.0 convolution_bitcast_fusion.2
  224.7 5.1 %fusion = bf16[1024,4224]{0,1:T(8,128)(2,1)} fusion(f32[1024,1408]{0,1:T(8,128)S(1)} %convolution_bitcast_fusion, f32[1024,1408]{0,1:T(8,128)S(1)} %convolution_bitcast_fusion.1, f32[1024,1408]{0,1:T(8,128)S(1)} %convolution_bitcast_fusion.2), kind=kLoop, calls=%fused_computation.1 | loop fusion | flops 17301504 | bytes 25952256 | tf_op jit(solution)/shard_map/convert_element_type | solution.py:9
  229.8 0.0 reduce-scatter.5.cloned.1.call-update
  229.8 0.0 all-reduce.2.cloned.1.call-start
  229.9 86.8 %reduce-scatter.5.cloned.1.call-done = bf16[256,4224]{0,1:T(8,128)(2,1)} async-done(((bf16[1024,4224]{0,1:T(8,128)(2,1)}), bf16[256,4224]{0,1:T(8,128)(2,1)}) %reduce-scatter.5.cloned.1.call-update) | async-done | bytes 2162704 | tf_op jit(solution)/shard_map/reduce_scatter | solution.py:9
  316.7 0.0 all-reduce.2.cloned.1.call-update
  316.7 0.0 copy-start.6
  316.7 0.0 reduce-scatter.3.cloned.1.call-start
  316.7 0.0 copy-start.3
  316.8 2.3 fusion.12
  319.1 0.0 copy-done.6
  319.1 0.0 copy-done.3
  319.1 1.9 fusion.7
  320.9 0.0 reduce-scatter.3.cloned.1.call-update
  321.0 85.7 %all-reduce.2.cloned.1.call-done = bf16[256,4224]{0,1:T(8,128)(2,1)} async-done(((bf16[256,4224]{0,1:T(8,128)(2,1)}), bf16[256,4224]{0,1:T(8,128)(2,1)}) %all-reduce.2.cloned.1.call-update) | async-done | bytes 2162704 | tf_op jit(solution)/shard_map/psum | solution.py:100
  406.7 2.6 fusion.11
  409.3 1.5 copy.20
  410.9 0.0 copy-start.4
  410.9 3.0 copy.19
  413.9 0.0 copy-done.4
  413.9 0.0 copy-start.1
  413.9 0.3 convert_element_type.66
  414.3 1.2 slice_bitcast_fusion
  415.5 1.1 reduce-scatter.3.cloned.1.call-done
  416.6 0.0 copy-done.1
Async XLA Ops:
  7.2 1.1 copy-start
  7.2 5.6 %copy-start.9 = (bf16[96,1024]{1,0:T(8,128)(2,1)S(1)}, bf16[96,1024]{1,0:T(8,128)(2,1)}, u32[]{:S(2)}) copy-start(bf16[96,1024]{1,0:T(8,128)(2,1)} %param.5) | copy-start | bytes 589828
  7.2 7.9 %copy-start.10 = (bf16[96,1024]{1,0:T(8,128)(2,1)S(1)}, bf16[96,1024]{1,0:T(8,128)(2,1)}, u32[]{:S(2)}) copy-start(bf16[96,1024]{1,0:T(8,128)(2,1)} %param.6) | copy-start | bytes 589828
  7.2 73.2 %all-gather.8.cloned.1.call-start = ((), (), s32[]{:S(2)}) async-start(), calls=%async_computation.4 | async-start | bytes 3063808 | tf_op jit(solution)/shard_map/all_gather | solution.py:51
  9.0 139.4 %all-gather.6.cloned.1.call-start = ((), (), s32[]{:S(2)}) async-start(), calls=%async_computation.3 | async-start | bytes 3063808 | tf_op jit(solution)/shard_map/all_gather | solution.py:52
  10.7 205.8 %all-gather.4.cloned.1.call-start = ((), (), s32[]{:S(2)}) async-start(), calls=%async_computation.2 | async-start | bytes 3063808 | tf_op jit(solution)/shard_map/all_gather | solution.py:53
  12.7 303.9 %reduce-scatter.5.cloned.1.call-start = ((), (), s32[]{:S(2)}) async-start(), calls=%async_computation.6 | async-start | bytes 10813440 | tf_op jit(solution)/shard_map/reduce_scatter | solution.py:9
  216.4 2.7 copy-start.2
  219.9 1.0 copy-start.8
  222.8 1.0 copy-start.5
  222.8 1.0 copy-start.7
  229.8 176.8 %all-reduce.2.cloned.1.call-start = ((), (), s32[]{:S(2)}) async-start(), calls=%async_computation.7 | async-start | bytes 4325376 | tf_op jit(solution)/shard_map/psum | solution.py:100
  316.7 2.4 copy-start.6
  316.7 99.9 %reduce-scatter.3.cloned.1.call-start = ((), (), s32[]{:S(2)}) async-start(), calls=%async_computation.5 | async-start | bytes 589824 | tf_op jit(solution)/shard_map/reduce_scatter | solution.py:9
  316.7 2.3 copy-start.3
  410.9 3.1 copy-start.4
  413.9 2.7 copy-start.1
Sparse Core Ops, SparseCore 0:
  11.3 69.0 all-gather.7
  83.7 64.6 all-gather.5
  151.7 64.6 all-gather.3
  230.0 86.6 reduce-scatter.4
  318.9 87.7 all-reduce.1
  409.4 7.2 reduce-scatter.2
where the time goes:
time: 424 us; the launch traced here: 423 us
  waiting for transfers between devices  367 us (87%)
  local copies, waits for them, and re-layouts  22.4 us (5%)
  between operations  14.3 us (3%)
  matrix products  9.49 us (2%)
  other arithmetic  5.43 us (1%)
  blocking collectives  4.44 us (1%)
    reduce_scatter x2, waiting for transfers between devices, summed_rows(): lax.psum_scatter(everything.astype(jnp.bfloat16), axis, scatter_dimension...  87.9 us
    psum x1, waiting for transfers between devices, body(): summed = lax.psum(owned.astype(jnp.bfloat16), 'rep').astype(jnp.float32)  85.7 us
    all_gather x1, waiting for transfers between devices, body(): lax.all_gather(pieces[1], ('rep', 'fs'), axis=0, tiled=True)  65.9 us
    all_gather x1, waiting for transfers between devices, body(): lax.all_gather(pieces[2], ('rep', 'fs'), axis=1, tiled=True)  64.4 us
    all_gather x1, waiting for transfers between devices, body(): lax.all_gather(pieces[0], ('rep', 'fs'), axis=0, tiled=True)  63.1 us
  transfers between devices with their start and end apart: 6, of which 6 were waited for; matrix products, arithmetic and copies ran while one was open for 5% of the time, Pallas kernels for 0%

commit v1 on v0

v1 whole, which is shorter than its diff:
```python
import jax
import jax.numpy as jnp
from jax import lax
from jax.sharding import PartitionSpec as P


def contract_last(left, right):
    return lax.dot_general(
        left, right, (((1,), (1,)), ((), ())), preferred_element_type=jnp.float32
    )


def contract_first(left, right):
    return lax.dot_general(
        left, right, (((0,), (0,)), ((), ())), preferred_element_type=jnp.float32
    )


def body(tokens_in, out_grad, gate_weight, up_weight, down_weight):
    replicas = lax.axis_size("rep")
    shards = lax.axis_size("fs")
    columns = lax.axis_size("tp")
    local_rows = tokens_in.shape[0]
    hidden_cols = gate_weight.shape[1]
    factor = (local_rows * replicas * shards * columns) ** (-0.5)
    part = hidden_cols // replicas
    offset = lax.axis_index("rep") * part
    pieces = jnp.stack(
        [
            lax.dynamic_slice_in_dim(gate_weight, offset, part, 1).T,
            lax.dynamic_slice_in_dim(up_weight, offset, part, 1).T,
            lax.dynamic_slice_in_dim(down_weight, offset, part, 0),
        ]
    )
    full = lax.all_gather(pieces, "fs", axis=2, tiled=True)
    gate_full, up_full, down_full = full[0], full[1], full[2]
    both = lax.all_gather(jnp.stack([tokens_in, out_grad]), ("rep", "tp"), axis=1, tiled=True)
    tokens_all, grads_all = both[0], both[1]
    gate = contract_last(tokens_all, gate_full).astype(jnp.bfloat16)
    up_proj = contract_last(tokens_all, up_full).astype(jnp.bfloat16)
    gate_wide = gate.astype(jnp.float32)
    up_wide = up_proj.astype(jnp.float32)
    sigmoid = jax.nn.sigmoid(gate_wide)
    activated = gate_wide * sigmoid
    hidden = (activated * up_wide).astype(jnp.bfloat16)
    grad_hidden = contract_last(grads_all, down_full).astype(jnp.bfloat16)
    grad_wide = grad_hidden.astype(jnp.float32)
    grad_gate = (grad_wide * up_wide * sigmoid * (1.0 + gate_wide * (1.0 - sigmoid))).astype(
        jnp.bfloat16
    )
    grad_up = (grad_wide * activated).astype(jnp.bfloat16)
    weights = factor * jnp.stack(
        [
            contract_first(grad_gate, tokens_all),
            contract_first(grad_up, tokens_all),
            contract_first(hidden, grads_all),
        ]
    )
    owned = lax.psum_scatter(
        weights.astype(jnp.bfloat16), "fs", scatter_dimension=2, tiled=True
    )
    summed = lax.all_gather(owned, "rep", axis=1, tiled=True).astype(jnp.float32)
    partial = jnp.dot(grad_gate, gate_full, preferred_element_type=jnp.float32) + jnp.dot(
        grad_up, up_full, preferred_element_type=jnp.float32
    )
    grad_in = lax.psum_scatter(
        partial.astype(jnp.bfloat16), ("rep", "tp"), scatter_dimension=0, tiled=True
    )
    return (grad_in, summed[0].T, summed[1].T, summed[2])


def solution(mesh):
    placed = (
        P(("rep", "fs", "tp"), None),
        P(("rep", "fs", "tp"), None),
        P("fs", "tp"),
        P("fs", "tp"),
        P("tp", "fs"),
    )
    return jax.shard_map(
        body,
        mesh=mesh,
        in_specs=placed,
        out_specs=(P(("rep", "fs", "tp"), None), P("fs", "tp"), P("fs", "tp"), P("tp", "fs")),
        check_vma=False,
    )
```

time: 424 us -> 225 us (0.53)
  waiting for transfers between devices: 367 us -> 183 us
  local copies, waits for them, and re-layouts: 22.4 us -> 9.15 us
  blocking collectives: 4.44 us -> 0 us
    psum x1 -> x0, waiting for transfers between devices: 85.7 us -> none  [body(): summed = lax.psum(owned.astype(jnp.bfloat16), 'rep').astype(jnp.float32)]
    all_gather x3, waiting for transfers between devices: 193 us -> 120 us  [the longest x1 43 us: body(): lax.all_gather(owned, 'rep', axis=1, tiled=True).astype(jnp.float32)]
    reduce_scatter x2, waiting for transfers between devices: 87.9 us -> 62.4 us  [the longest x1 34.8 us: body(): lax.psum_scatter(weights.astype(jnp.bfloat16), 'fs', scatter_dimension=2,...]
    transpose x4 -> x0, local copies, waits for them, and re-layouts: 9.14 us -> none  [the longest x3 7.94 us: regroup(): return jnp.transpose(block.reshape(new_shape), layout).reshape(old_shape)]
    all_gather x2 -> x0, blocking collectives: 4.44 us -> none  [the longest x1 2.23 us: body(): lax.all_gather(tokens_in, 'tp', axis=0, tiled=True)]
  transfers between devices with their start and end apart: 6 -> 5, of which waited for: 6 -> 5; matrix products, arithmetic and copies ran while one was open for 5% -> 6% of each run, Pallas kernels for 0% -> 0%
where the time goes in v1:
time: 225 us
  waiting for transfers between devices  183 us (81%)
  between operations  14 us (6%)
  matrix products  13 us (6%)
  local copies, waits for them, and re-layouts  9.15 us (4%)
  other arithmetic  5.58 us (2%)
    all_gather x1, waiting for transfers between devices, body(): lax.all_gather(owned, 'rep', axis=1, tiled=True).astype(jnp.float32)  43 us
    all_gather x1, waiting for transfers between devices, body(): lax.all_gather(jnp.stack([tokens_in, out_grad]), ('rep', 'tp'), axis=1, t...  40.1 us
    all_gather x1, waiting for transfers between devices, body(): full = lax.all_gather(pieces, 'fs', axis=2, tiled=True)  37.4 us
    reduce_scatter x1, waiting for transfers between devices, body(): lax.psum_scatter(weights.astype(jnp.bfloat16), 'fs', scatter_dimension=2,...  34.8 us
    reduce_scatter x1, waiting for transfers between devices, body(): lax.psum_scatter(partial.astype(jnp.bfloat16), ('rep', 'tp'), scatter_dim...  27.6 us
    unnamed x20, local copies, waits for them, and re-layouts  5.87 us
    dot_general x3, matrix products, contract_last(): lax.dot_general(left, right, (((1,), (1,)), ((), ())), preferred_element_...  5.43 us
  transfers between devices with their start and end apart: 5, of which 5 were waited for; matrix products, arithmetic and copies ran while one was open for 6% of the time, Pallas kernels for 0%

profile of v1, /device:TPU:0, one launch (start us, length us, event | category | flops | bytes accessed | tf_op | source)
XLA Modules:
  0.0 224.8 jit_solution(11727370553388090820)
XLA Ops:
  7.2 0.0 copy-start
  7.2 0.0 all-gather.6.cloned.1.call-start
  7.2 1.0 copy-done
  8.3 0.0 copy-start.1
  8.3 0.0 copy-start.2
  8.3 1.3 constant_dynamic-slice_fusion
  9.6 0.1 copy.16
  9.8 0.1 copy.15
  9.9 0.9 pad_maximum_fusion
  10.8 0.0 all-gather.6.cloned.1.call-update
  10.8 0.0 all-gather.4.cloned.1.call-start
  10.8 0.0 copy-done.1
  10.8 0.0 copy-done.2
  10.9 0.8 pad_maximum_fusion.1
  11.6 0.0 all-gather.4.cloned.1.call-update
  11.7 0.0 reduce-scatter.5.cloned.1.call-start
  11.7 37.4 %all-gather.6.cloned.1.call-done = bf16[3,352,1024]{2,1,0:T(8,128)(2,1)} async-done(((bf16[3,352,256]{2,1,0:T(8,128)(2,1)}), bf16[3,352,1024]{2,1,0:T(8,128)(2,1)}) %all-gather.6.cloned.1.call-update) | async-done | bytes 2162704 | tf_op jit(solution)/shard_map/all_gather | solution.py:35
  49.1 40.1 %all-gather.4.cloned.1.call-done = bf16[2,768,1024]{2,1,0:T(8,128)(2,1)} async-done(((bf16[2,96,1024]{2,1,0:T(8,128)(2,1)}), bf16[2,768,1024]{2,1,0:T(8,128)(2,1)}) %all-gather.4.cloned.1.call-update) | async-done | bytes 3145744 | tf_op jit(solution)/shard_map/all_gather | solution.py:37
  89.2 0.0 copy-start.3
  89.2 2.5 %convolution_convert_fusion.1 = bf16[768,352]{0,1:T(8,128)(2,1)S(1)} fusion(bf16[2,768,1024]{2,1,0:T(8,128)(2,1)} %all-gather.4.cloned.1.call-done, bf16[3,352,1024]{2,1,0:T(8,128)(2,1)} %all-gather.6.cloned.1.call-done), kind=kOutput, calls=%fused_computation.20 | convolution fusion | flops 553918464 | bytes 2834432 | tf_op jit(solution)/shard_map/dot_general | solution.py:8
  91.7 0.1 copy-done.3
  91.8 0.0 copy-start.7
  91.8 0.0 copy-start.4
  91.8 2.2 fusion.2
  94.0 0.0 copy-done.4
  94.0 0.8 convolution_convert_fusion
  94.8 0.0 copy-start.5
  94.8 0.8 convolution_bitcast_fusion
  95.6 0.9 convolution_bitcast_fusion.1
  96.5 0.0 copy-done.7
  96.5 0.0 copy-done.5
  96.5 1.0 convolution_bitcast_fusion.2
  97.5 2.0 fusion
  99.5 0.0 reduce-scatter.5.cloned.1.call-update
  99.5 0.0 all-gather.8.cloned.1.call-start
  99.5 34.8 %reduce-scatter.5.cloned.1.call-done = bf16[3,352,256]{2,1,0:T(8,128)(2,1)} async-done(((bf16[3,352,1024]{2,1,0:T(8,128)(2,1)}), bf16[3,352,256]{2,1,0:T(8,128)(2,1)}) %reduce-scatter.5.cloned.1.call-update) | async-done | bytes 540688 | tf_op jit(solution)/shard_map/reduce_scatter | solution.py:59
  134.4 0.0 all-gather.8.cloned.1.call-update
  134.4 0.0 reduce-scatter.3.cloned.1.call-start
  134.5 0.0 copy-start.6
  134.5 2.5 %fusion.12 = f32[768,1024]{1,0:T(8,128)S(1)} fusion(bf16[3,352,1024]{2,1,0:T(8,128)(2,1)S(1)} %copy-done.4, bf16[768,352]{0,1:T(8,128)(2,1)} %copy-done.7, bf16[768,352]{0,1:T(8,128)(2,1)S(1)} %fusion.2, bf16[768,352]{0,1:T(8,128)(2,1)} %copy-done.5), kind=kOutput, calls=%fused_computation.33 | convolution fusion | flops 557162496 | bytes 5488640 | tf_op jit(solution)/shard_map/dot_general | solution.py:63
  137.0 0.0 copy-done.6
  137.0 2.3 %add_convert_fusion = bf16[768,1024]{1,0:T(8,128)(2,1)} fusion(f32[768,1024]{1,0:T(8,128)S(1)} %fusion.12, bf16[3,352,1024]{2,1,0:T(8,128)(2,1)S(1)} %copy-done.4, bf16[768,352]{0,1:T(8,128)(2,1)S(1)} %fusion.2, bf16[768,352]{0,1:T(8,128)(2,1)S(1)} %copy-done.6), kind=kOutput, calls=%fused_computation.2 | convolution fusion | flops 557383680 | bytes 6520832 | tf_op jit(solution)/shard_map/dot_general | solution.py:63
  139.3 0.0 reduce-scatter.3.cloned.1.call-update
  139.4 43.0 %all-gather.8.cloned.1.call-done = bf16[3,1408,256]{2,1,0:T(8,128)(2,1)} async-done(((bf16[3,352,256]{2,1,0:T(8,128)(2,1)}), bf16[3,1408,256]{2,1,0:T(8,128)(2,1)}) %all-gather.8.cloned.1.call-update) | async-done | bytes 2162704 | tf_op jit(solution)/shard_map/all_gather | solution.py:62
  182.4 2.0 convert_element_type.47
  184.3 2.0 slice_bitcast_fusion.2
  186.3 2.9 %copy.13 = f32[256,1408]{1,0:T(8,128)} copy(f32[256,1408]{0,1:T(8,128)} %get-tuple-element.14) | data formatting | bytes 2883584
  189.2 1.5 copy.14
  190.8 27.6 %reduce-scatter.3.cloned.1.call-done = bf16[96,1024]{1,0:T(8,128)(2,1)} async-done(((bf16[768,1024]{1,0:T(8,128)(2,1)}), bf16[96,1024]{1,0:T(8,128)(2,1)}) %reduce-scatter.3.cloned.1.call-update) | async-done | bytes 196624 | tf_op jit(solution)/shard_map/reduce_scatter | solution.py:66
  (1 shorter events, 0.0 us)
Async XLA Ops:
  7.2 1.1 copy-start
  7.2 41.9 %all-gather.6.cloned.1.call-start = ((), (), s32[]{:S(2)}) async-start(), calls=%async_computation.3 | async-start | bytes 2703360 | tf_op jit(solution)/shard_map/all_gather | solution.py:35
  8.3 2.5 %copy-start.1 = (bf16[96,1024]{1,0:T(8,128)(2,1)S(1)}, bf16[96,1024]{1,0:T(8,128)(2,1)}, u32[]{:S(2)}) copy-start(bf16[96,1024]{1,0:T(8,128)(2,1)} %param.6) | copy-start | bytes 589828
  8.3 2.5 %copy-start.2 = (bf16[96,1024]{1,0:T(8,128)(2,1)S(1)}, bf16[96,1024]{1,0:T(8,128)(2,1)}, u32[]{:S(2)}) copy-start(bf16[96,1024]{1,0:T(8,128)(2,1)} %param.5) | copy-start | bytes 589828
  10.8 78.4 %all-gather.4.cloned.1.call-start = ((), (), s32[]{:S(2)}) async-start(), calls=%async_computation.2 | async-start | bytes 3538944 | tf_op jit(solution)/shard_map/all_gather | solution.py:37
  11.7 122.7 %reduce-scatter.5.cloned.1.call-start = ((), (), s32[]{:S(2)}) async-start(), calls=%async_computation.5 | async-start | bytes 2703360 | tf_op jit(solution)/shard_map/reduce_scatter | solution.py:59
  89.2 2.6 %copy-start.3 = (bf16[2,768,1024]{2,1,0:T(8,128)(2,1)S(1)}, bf16[2,768,1024]{2,1,0:T(8,128)(2,1)}, u32[]{:S(2)}) copy-start(bf16[2,768,1024]{2,1,0:T(8,128)(2,1)} %all-gather.4.cloned.1.call-done) | copy-start | bytes 9437188
  91.8 4.7 %copy-start.7 = (bf16[768,352]{0,1:T(8,128)(2,1)}, bf16[768,352]{0,1:T(8,128)(2,1)S(1)}, u32[]{:S(2)}) copy-start(bf16[768,352]{0,1:T(8,128)(2,1)S(1)} %convolution_convert_fusion.1) | copy-start | bytes 1622020
  91.8 2.2 copy-start.4
  94.8 1.7 copy-start.5
  99.5 82.9 %all-gather.8.cloned.1.call-start = ((), (), s32[]{:S(2)}) async-start(), calls=%async_computation.6 | async-start | bytes 2703360 | tf_op jit(solution)/shard_map/all_gather | solution.py:62
  134.4 83.9 %reduce-scatter.3.cloned.1.call-start = ((), (), s32[]{:S(2)}) async-start(), calls=%async_computation.4 | async-start | bytes 1769472 | tf_op jit(solution)/shard_map/reduce_scatter | solution.py:66
  134.5 2.6 %copy-start.6 = (bf16[768,352]{0,1:T(8,128)(2,1)S(1)}, bf16[768,352]{0,1:T(8,128)(2,1)}, u32[]{:S(2)}) copy-start(bf16[768,352]{0,1:T(8,128)(2,1)} %copy-done.5) | copy-start | bytes 1622020
Sparse Core Ops, SparseCore 0:
  10.9 38.1 all-gather.5
  51.2 37.9 all-gather.3
  99.6 34.7 reduce-scatter.4
  135.8 46.5 all-gather.7
  185.1 33.1 reduce-scatter.2

commit v2 on v1

--- a/solution.py
+++ b/solution.py
@@ -1,7 +1,331 @@
+import functools
+
 import jax
 import jax.numpy as jnp
 from jax import lax
+from jax.experimental import pallas as pl
+from jax.experimental.pallas import tpu as pltpu
 from jax.sharding import PartitionSpec as P
+
+BF = jnp.bfloat16
+F32 = jnp.float32
+MESH = pl.DeviceIdType.MESH
+
+
+def ring_order(index):
+    return index + (index // 2) * (5 - 2 * index)
+
+
+def kernel(
+    columns,
+    factor,
+    tokens_ref,
+    grads_ref,
+    w_ref,
+    gin_ref,
+    gw_ref,
+    T,
+    W,
+    H,
+    S,
+    O,
+    RD,
+    RR,
+    G,
+    PS,
+    PR,
+    Q,
+    QR,
+    w_send,
+    w_recv,
+    t_send,
+    t_recv,
+    c_send,
+    c_recv,
+    d_send,
+    d_recv,
+    s_send,
+    s_recv,
+    g_send,
+    g_recv,
+    p_send,
+    p_recv,
+    q_send,
+    q_recv,
+):
+    rep = lax.axis_index("rep")
+    fs = lax.axis_index("fs")
+    tp = lax.axis_index("tp")
+    rows = tokens_ref.shape[0]
+    width = w_ref.shape[2]
+    half = width // 2
+    tile = 4 * rows
+    spot = ring_order(fs)
+    near = [ring_order(lax.rem(spot + k, 4)) for k in range(4)]
+    level = [lax.rem(rep + k, 4) for k in range(4)]
+    core = [lax.rem(tp + k, columns) for k in range(columns)]
+
+    def to_fs(k):
+        return (rep, near[k], tp)
+
+    def to_rep(k):
+        return (level[k], fs, tp)
+
+    def to_tp(k):
+        return (rep, fs, core[k])
+
+    peers = [to_fs(k) for k in (1, 2, 3)] + [to_rep(k) for k in (1, 2, 3)]
+    peers += [to_tp(k) for k in range(1, columns)]
+    barrier = pltpu.get_barrier_semaphore()
+    for peer in peers:
+        pl.semaphore_signal(barrier, inc=1, device_id=peer, device_id_type=MESH)
+    pl.semaphore_wait(barrier, len(peers))
+
+    pending = []
+
+    def send(src, dst, send_sem, recv_sem, device):
+        copy = pltpu.make_async_remote_copy(
+            src_ref=src, dst_ref=dst, send_sem=send_sem, recv_sem=recv_sem,
+            device_id=device, device_id_type=MESH,
+        )
+        copy.start()
+        pending.append(copy)
+
+    def arrive(dst, send_sem, recv_sem, device):
+        pltpu.make_async_remote_copy(
+            src_ref=dst, dst_ref=dst, send_sem=send_sem, recv_sem=recv_sem,
+            device_id=device, device_id_type=MESH,
+        ).wait_recv()
+
+    sides = (1, 3)
+
+    def lanes(side):
+        return pl.ds(side * half, half)
+
+    def block(kind, column, row):
+        start = pl.multiple_of((column * 4 + row) * rows, rows)
+        return T.at[kind, pl.ds(start, rows), :]
+
+    mine = (tokens_ref, grads_ref)
+    for kind in range(2):
+        for side in range(2):
+            send(mine[kind], block(kind, tp, rep), t_send.at[0, kind, side],
+                 t_recv.at[0, kind, side], to_rep(sides[side]))
+    for w in range(3):
+        for side in range(2):
+            send(w_ref.at[w], W.at[fs, w], w_send.at[0, w, side], w_recv.at[0, w, side],
+                 to_fs(sides[side]))
+
+    def share(kind, k):
+        for j in range(1, columns):
+            if k == 0:
+                src = mine[kind]
+            else:
+                src = block(kind, tp, level[k])
+            send(src, block(kind, tp, level[k]), c_send.at[j, kind, k], c_recv.at[j, kind, k],
+                 to_tp(j))
+
+    for kind in range(2):
+        share(kind, 0)
+        T[kind, pl.ds(pl.multiple_of((tp * 4 + rep) * rows, rows), rows), :] = mine[kind][...]
+    W[fs] = w_ref[...]
+
+    for kind in range(2):
+        for side in range(2):
+            k = 4 - sides[side]
+            arrive(block(kind, tp, level[k]), t_send.at[0, kind, side],
+                   t_recv.at[0, kind, side], to_rep(sides[side]))
+            if kind == side:
+                send(block(kind, tp, level[k]), block(kind, tp, level[k]),
+                     t_send.at[1, kind, side], t_recv.at[1, kind, side], to_rep(sides[side]))
+            share(kind, k)
+    for w in range(3):
+        for side in range(2):
+            f = near[4 - sides[side]]
+            arrive(W.at[f, w], w_send.at[0, w, side], w_recv.at[0, w, side], to_fs(sides[side]))
+            send(W.at[f, w, :, lanes(side)], W.at[f, w, :, lanes(side)],
+                 w_send.at[1, w, side], w_recv.at[1, w, side], to_fs(sides[side]))
+    for kind in range(2):
+        arrive(block(kind, tp, level[2]), t_send.at[1, kind, kind], t_recv.at[1, kind, kind],
+               to_rep(sides[kind]))
+        share(kind, 2)
+    for kind in range(2):
+        for k in range(4):
+            for j in range(1, columns):
+                arrive(block(kind, core[columns - j], level[k]), c_send.at[j, kind, k],
+                       c_recv.at[j, kind, k], to_tp(j))
+    for w in range(3):
+        for side in range(2):
+            arrive(W.at[near[2], w, :, lanes(side)], w_send.at[1, w, side],
+                   w_recv.at[1, w, side], to_fs(sides[side]))
+
+    def product(kind, w, at):
+        total = None
+        for f in range(4):
+            piece = lax.dot_general(
+                T[kind, at, f * width : (f + 1) * width], W[f, w],
+                (((1,), (1,)), ((), ())), preferred_element_type=F32,
+            )
+            total = piece if total is None else total + piece
+        return total.astype(BF).astype(F32)
+
+    def activations(i, carry):
+        at = pl.ds(pl.multiple_of(i * tile, tile), tile)
+        gate = product(0, 0, at)
+        up = product(0, 1, at)
+        sigmoid = jax.nn.sigmoid(gate)
+        activated = gate * sigmoid
+        H[2, at, :] = (activated * up).astype(BF)
+        grad = product(1, 2, at)
+        H[0, at, :] = (grad * up * sigmoid * (1.0 + gate * (1.0 - sigmoid))).astype(BF)
+        H[1, at, :] = (grad * activated).astype(BF)
+        return carry
+
+    lax.fori_loop(0, columns, activations, 0)
+
+    def weight_part(w, k):
+        at = pl.ds(pl.multiple_of(near[k] * width, width), width)
+        return factor * lax.dot_general(
+            H[w], T[1 if w == 2 else 0, :, at], (((0,), (0,)), ((), ())),
+            preferred_element_type=F32,
+        )
+
+    for w in range(3):
+        far = weight_part(w, 2).astype(BF)
+        for side in range(2):
+            S[w, 0, side] = far[:, side * half : (side + 1) * half]
+            send(S.at[w, 0, side], RD.at[w, side], d_send.at[w, side], d_recv.at[w, side],
+                 to_fs(sides[side]))
+        for side in range(2):
+            part = weight_part(w, sides[side]).astype(BF)
+            for h in range(2):
+                S[w, 1 + side, h] = part[:, h * half : (h + 1) * half]
+            h = 1 - side
+            send(S.at[w, 1 + side, h], RR.at[w, side, h], s_send.at[w, side, h],
+                 s_recv.at[w, side, h], to_fs(sides[side]))
+        O[w] = weight_part(w, 0)
+
+    def input_part(i, f):
+        at = pl.ds(pl.multiple_of(i * tile, tile), tile)
+        return jnp.dot(H[0, at, :], W[f, 0], preferred_element_type=F32) + jnp.dot(
+            H[1, at, :], W[f, 1], preferred_element_type=F32
+        )
+
+    for j in range(1, columns):
+        for f in range(4):
+            PS[j, :, f * width : (f + 1) * width] = input_part(core[j], f).astype(BF)
+        send(PS.at[j], PR.at[j], p_send.at[j], p_recv.at[j], to_tp(j))
+
+    for w in range(3):
+        for side in range(2):
+            arrive(RD.at[w, side], d_send.at[w, side], d_recv.at[w, side], to_fs(sides[side]))
+            S[w, 3 + side, side] = (
+                S[w, 1 + side, side].astype(F32) + RD[w, side].astype(F32)
+            ).astype(BF)
+            send(S.at[w, 3 + side, side], RR.at[w, side, side], s_send.at[w, side, side],
+                 s_recv.at[w, side, side], to_fs(sides[side]))
+
+    for j in range(1, columns):
+        arrive(PR.at[j], p_send.at[j], p_recv.at[j], to_tp(j))
+    for f in range(4):
+        at = slice(f * width, (f + 1) * width)
+        total = input_part(tp, f)
+        for j in range(1, columns):
+            total += PR[j, :, at].astype(F32)
+        for r in range(4):
+            Q[r, :, at] = total[r * rows : (r + 1) * rows].astype(BF)
+    for k in (2, 1, 3):
+        send(Q.at[level[k]], QR.at[k], q_send.at[k], q_recv.at[k], to_rep(k))
+
+    for w in range(3):
+        for side in range(2):
+            for h in range(2):
+                arrive(RR.at[w, side, h], s_send.at[w, side, h], s_recv.at[w, side, h],
+                       to_fs(sides[side]))
+        for h in range(2):
+            at = slice(h * half, (h + 1) * half)
+            G[rep, w, :, at] = (
+                O[w, :, at] + RR[w, 0, h].astype(F32) + RR[w, 1, h].astype(F32)
+            ).astype(BF)
+        for side in range(2):
+            send(G.at[rep, w], G.at[rep, w], g_send.at[0, w, side], g_recv.at[0, w, side],
+                 to_rep(sides[side]))
+
+    for k in (1, 2, 3):
+        arrive(QR.at[k], q_send.at[k], q_recv.at[k], to_rep(k))
+    total = Q[rep].astype(F32)
+    for k in (1, 2, 3):
+        total += QR[k].astype(F32)
+    gin_ref[...] = total.astype(BF)
+
+    for w in range(3):
+        for side in range(2):
+            r = level[4 - sides[side]]
+            arrive(G.at[r, w], g_send.at[0, w, side], g_recv.at[0, w, side], to_rep(sides[side]))
+            send(G.at[r, w, :, lanes(side)], G.at[r, w, :, lanes(side)],
+                 g_send.at[1, w, side], g_recv.at[1, w, side], to_rep(sides[side]))
+    for w in range(3):
+        for side in range(2):
+            arrive(G.at[level[2], w, :, lanes(side)], g_send.at[1, w, side],
+                   g_recv.at[1, w, side], to_rep(sides[side]))
+        for r in range(4):
+            gw_ref[w, r] = G[r, w]
+    for copy in pending:
+        copy.wait_send()
+
+
+def body(tokens_in, out_grad, gate_weight, up_weight, down_weight):
+    replicas = lax.axis_size("rep")
+    shards = lax.axis_size("fs")
+    columns = lax.axis_size("tp")
+    rows, model = tokens_in.shape
+    width, hidden_cols = gate_weight.shape
+    everyone = rows * replicas * columns
+    factor = (everyone * shards) ** (-0.5)
+    part = hidden_cols // replicas
+    half = width // 2
+    offset = lax.axis_index("rep") * part
+    pieces = jnp.stack(
+        [
+            lax.dynamic_slice_in_dim(gate_weight, offset, part, 1).T,
+            lax.dynamic_slice_in_dim(up_weight, offset, part, 1).T,
+            lax.dynamic_slice_in_dim(down_weight, offset, part, 0),
+        ]
+    )
+    sems = pltpu.SemaphoreType.DMA
+    shapes = []
+    for dims in ((2, 3, 2), (2, 2, 2), (columns, 2, 4), (3, 2), (3, 2, 2), (2, 3, 2), (columns,), (4,)):
+        shapes += [sems(dims), sems(dims)]
+    vmem = pl.BlockSpec(memory_space=pltpu.VMEM)
+    grad_in, summed = pl.pallas_call(
+        functools.partial(kernel, columns, factor),
+        out_shape=(
+            jax.ShapeDtypeStruct((rows, model), BF),
+            jax.ShapeDtypeStruct((3, 4, part, width), BF),
+        ),
+        in_specs=[vmem] * 3,
+        out_specs=(vmem, vmem),
+        scratch_shapes=[
+            pltpu.VMEM((2, everyone, model), BF),
+            pltpu.VMEM((4, 3, part, width), BF),
+            pltpu.VMEM((3, everyone, part), BF),
+            pltpu.VMEM((3, 5, 2, part, half), BF),
+            pltpu.VMEM((3, part, width), F32),
+            pltpu.VMEM((3, 2, part, half), BF),
+            pltpu.VMEM((3, 2, 2, part, half), BF),
+            pltpu.VMEM((4, 3, part, width), BF),
+            pltpu.VMEM((columns, 4 * rows, model), BF),
+            pltpu.VMEM((columns, 4 * rows, model), BF),
+            pltpu.VMEM((4, rows, model), BF),
+            pltpu.VMEM((4, rows, model), BF),
+        ]
+        + shapes,
+        compiler_params=pltpu.CompilerParams(
+            collective_id=0, has_side_effects=True, vmem_limit_bytes=60 * 1024 * 1024
+        ),
+    )(tokens_in, out_grad, pieces)
+    wide = summed.reshape(3, hidden_cols, width).astype(F32)
+    return (grad_in, wide[0].T, wide[1].T, wide[2])
 
 
 def contract_last(left, right):
@@ -16,7 +340,7 @@
     )
 
 
-def body(tokens_in, out_grad, gate_weight, up_weight, down_weight):
+def plain_body(tokens_in, out_grad, gate_weight, up_weight, down_weight):
     replicas = lax.axis_size("rep")
     shards = lax.axis_size("fs")
     columns = lax.axis_size("tp")
@@ -77,8 +401,9 @@
         P("fs", "tp"),
         P("tp", "fs"),
     )
+    fits = mesh.shape["rep"] == 4 and mesh.shape["fs"] == 4
     return jax.shard_map(
-        body,
+        body if fits else plain_body,
         mesh=mesh,
         in_specs=placed,
         out_specs=(P(("rep", "fs", "tp"), None), P("fs", "tp"), P("fs", "tp"), P("tp", "fs")),

time: 225 us -> 117 us (0.52)
  the two profiles are of different devices: /device:TPU:0 before, /device:TPU:9 now
where the time goes in v2:
time: 117 us
  Pallas kernels  104 us (89%)
  local copies, waits for them, and re-layouts  11.3 us (10%)
    pallas_call x1, Pallas kernels, body(): pl.pallas_call(functools.partial(kernel, columns, factor), out_shape=(jax...  104 us
    squeeze x2, local copies, waits for them, and re-layouts, body(): return (grad_in, wide[0].T, wide[1].T, wide[2])  4.43 us
    slice x1, local copies, waits for them, and re-layouts, body(): return (grad_in, wide[0].T, wide[1].T, wide[2])  3.53 us

profile of v2, /device:TPU:9, one launch (start us, length us, event | category | flops | bytes accessed | tf_op | source)
XLA Modules:
  0.0 116.9 jit_solution(6439516926688736899)
XLA Ops:
  0.6 0.0 copy-start
  0.7 1.1 copy-done
  1.8 1.2 %constant_dynamic-slice_fusion = (bf16[256,352]{1,0:T(8,128)(2,1)S(1)}, bf16[256,352]{1,0:T(8,128)(2,1)S(1)}) fusion(bf16[256,1408]{1,0:T(8,128)(2,1)} %param.8, s32[]{:T(128)S(6)} %select_n.2, bf16[256,1408]{1,0:T(8,128)(2,1)} %param.7), kind=kLoop, calls=%fused_computation.2 | loop fusion | bytes 720900 | tf_op jit(solution)/shard_map/dynamic_slice | solution.py:291
  3.0 0.1 copy.14
  3.2 0.1 copy.13
  3.3 0.9 pad_maximum_fusion.w_ref
  4.2 104.1 %shard_map.84 = (bf16[96,1024]{1,0:T(8,128)(2,1)}, bf16[3,4,352,256]{3,2,1,0:T(8,128)(2,1)}) custom-call(bf16[96,1024]{1,0:T(8,128)(2,1)} %tokens_ref.1, bf16[96,1024]{1,0:T(8,128)(2,1)} %grads_ref.1, bf16[3,352,256]{2,1,0:T(8,128)(2,1)} %pad_maximum_fusion.w_ref), custom_call_target="tpu_custom_call" | custom-call | tf_op jit(solution)/shard_map/pallas_call | solution.py:300
  108.3 3.5 %fusion = (f32[1,4,352,256]{3,2,1,0:T(8,128)}, f32[1,4,352,256]{3,2,1,0:T(8,128)}, f32[1,4,352,256]{3,2,1,0:T(8,128)S(1)}) fusion(bf16[3,4,352,256]{3,2,1,0:T(8,128)(2,1)} %get-tuple-element.7), kind=kLoop, calls=%fused_computation.4 | loop fusion | bytes 8650752 | tf_op jit(solution)/shard_map/slice | solution.py:328
  111.8 2.9 %copy.12 = f32[1408,256]{0,1:T(8,128)} copy(f32[1408,256]{1,0:T(8,128)} %bitcast.14) | data formatting | bytes 2883584 | tf_op jit(solution)/shard_map/squeeze | solution.py:328
  114.7 0.0 copy-start.1
  114.7 1.5 %copy.11 = f32[1408,256]{0,1:T(8,128)} copy(f32[1408,256]{1,0:T(8,128)S(1)} %bitcast.13) | data formatting | bytes 2883584 | tf_op jit(solution)/shard_map/squeeze | solution.py:328
  116.2 0.0 copy-done.1
  116.2 0.7 copy.16
  (1 shorter events, 0.0 us)
Async XLA Ops:
  0.6 1.1 copy-start
  114.7 1.5 %copy-start.1 = (bf16[96,1024]{1,0:T(8,128)(2,1)S(1)}, bf16[96,1024]{1,0:T(8,128)(2,1)}, u32[]{:S(2)}) copy-start(bf16[96,1024]{1,0:T(8,128)(2,1)} %get-tuple-element.17) | copy-start | bytes 589828

commit v3 on v2

--- a/solution.py
+++ b/solution.py
@@ -23,7 +23,8 @@
     grads_ref,
     w_ref,
     gin_ref,
-    gw_ref,
+    gu_ref,
+    gd_ref,
     T,
     W,
     H,
@@ -58,6 +59,7 @@
     tp = lax.axis_index("tp")
     rows = tokens_ref.shape[0]
     width = w_ref.shape[2]
+    part = w_ref.shape[1]
     half = width // 2
     tile = 4 * rows
     spot = ring_order(fs)
@@ -190,7 +192,7 @@
             preferred_element_type=F32,
         )
 
-    for w in range(3):
+    def scatter(w):
         far = weight_part(w, 2).astype(BF)
         for side in range(2):
             S[w, 0, side] = far[:, side * half : (side + 1) * half]
@@ -216,15 +218,7 @@
             PS[j, :, f * width : (f + 1) * width] = input_part(core[j], f).astype(BF)
         send(PS.at[j], PR.at[j], p_send.at[j], p_recv.at[j], to_tp(j))
 
-    for w in range(3):
-        for side in range(2):
-            arrive(RD.at[w, side], d_send.at[w, side], d_recv.at[w, side], to_fs(sides[side]))
-            S[w, 3 + side, side] = (
-                S[w, 1 + side, side].astype(F32) + RD[w, side].astype(F32)
-            ).astype(BF)
-            send(S.at[w, 3 + side, side], RR.at[w, side, side], s_send.at[w, side, side],
-                 s_recv.at[w, side, side], to_fs(sides[side]))
-
+    scatter(0)
     for j in range(1, columns):
         arrive(PR.at[j], p_send.at[j], p_recv.at[j], to_tp(j))
     for f in range(4):
@@ -237,6 +231,18 @@
     for k in (2, 1, 3):
         send(Q.at[level[k]], QR.at[k], q_send.at[k], q_recv.at[k], to_rep(k))
 
+    scatter(1)
+    scatter(2)
+
+    for w in range(3):
+        for side in range(2):
+            arrive(RD.at[w, side], d_send.at[w, side], d_recv.at[w, side], to_fs(sides[side]))
+            S[w, 3 + side, side] = (
+                S[w, 1 + side, side].astype(F32) + RD[w, side].astype(F32)
+            ).astype(BF)
+            send(S.at[w, 3 + side, side], RR.at[w, side, side], s_send.at[w, side, side],
+                 s_recv.at[w, side, side], to_fs(sides[side]))
+
     for w in range(3):
         for side in range(2):
             for h in range(2):
@@ -269,7 +275,10 @@
             arrive(G.at[level[2], w, :, lanes(side)], g_send.at[1, w, side],
                    g_recv.at[1, w, side], to_rep(sides[side]))
         for r in range(4):
-            gw_ref[w, r] = G[r, w]
+            if w == 2:
+                gd_ref[r] = G[r, w]
+            else:
+                gu_ref[w, :, r * part : (r + 1) * part] = G[r, w].astype(F32).T.astype(BF)
     for copy in pending:
         copy.wait_send()
 
@@ -297,14 +306,15 @@
     for dims in ((2, 3, 2), (2, 2, 2), (columns, 2, 4), (3, 2), (3, 2, 2), (2, 3, 2), (columns,), (4,)):
         shapes += [sems(dims), sems(dims)]
     vmem = pl.BlockSpec(memory_space=pltpu.VMEM)
-    grad_in, summed = pl.pallas_call(
+    grad_in, wide, down = pl.pallas_call(
         functools.partial(kernel, columns, factor),
         out_shape=(
             jax.ShapeDtypeStruct((rows, model), BF),
-            jax.ShapeDtypeStruct((3, 4, part, width), BF),
+            jax.ShapeDtypeStruct((2, width, hidden_cols), BF),
+            jax.ShapeDtypeStruct((4, part, width), BF),
         ),
         in_specs=[vmem] * 3,
-        out_specs=(vmem, vmem),
+        out_specs=(vmem, vmem, vmem),
         scratch_shapes=[
             pltpu.VMEM((2, everyone, model), BF),
             pltpu.VMEM((4, 3, part, width), BF),
@@ -324,8 +334,12 @@
             collective_id=0, has_side_effects=True, vmem_limit_bytes=60 * 1024 * 1024
         ),
     )(tokens_in, out_grad, pieces)
-    wide = summed.reshape(3, hidden_cols, width).astype(F32)
-    return (grad_in, wide[0].T, wide[1].T, wide[2])
+    return (
+        grad_in,
+        wide[0].astype(F32),
+        wide[1].astype(F32),
+        down.reshape(hidden_cols, width).astype(F32),
+    )
 
 
 def contract_last(left, right):

time: 117 us -> 105 us (0.90)
  the two profiles are of different devices: /device:TPU:9 before, /device:TPU:0 now
where the time goes in v3:
time: 105 us; the launch traced here: 104 us
  Pallas kernels  95.6 us (91%)
  other arithmetic  5.28 us (5%)
  local copies, waits for them, and re-layouts  2.3 us (2%)
    pallas_call x1, Pallas kernels, body(): pl.pallas_call(functools.partial(kernel, columns, factor), out_shape=(jax...  95.6 us
    convert_element_type x1, other arithmetic, body(): wide[1].astype(F32)  3.17 us

profile of v3, /device:TPU:0, one launch (start us, length us, event | category | flops | bytes accessed | tf_op | source)
XLA Modules:
  0.0 103.9 jit_solution(16030838204751616253)
XLA Ops:
  0.6 0.0 copy-start
  0.7 1.3 %constant_dynamic-slice_fusion = (bf16[256,352]{1,0:T(8,128)(2,1)S(1)}, bf16[256,352]{1,0:T(8,128)(2,1)S(1)}) fusion(bf16[256,1408]{1,0:T(8,128)(2,1)} %param.8, s32[]{:T(128)S(6)} %select_n.2, bf16[256,1408]{1,0:T(8,128)(2,1)} %param.7), kind=kLoop, calls=%fused_computation.5 | loop fusion | bytes 720900 | tf_op jit(solution)/shard_map/dynamic_slice | solution.py:300
  2.0 0.1 copy.11
  2.1 0.1 copy.12
  2.2 0.0 copy-done
  2.3 0.9 pad_maximum_fusion.w_ref
  3.1 95.6 %shard_map.84 = (bf16[96,1024]{1,0:T(8,128)(2,1)}, bf16[2,256,1408]{2,1,0:T(8,128)(2,1)}, bf16[4,352,256]{2,1,0:T(8,128)(2,1)}) custom-call(bf16[96,1024]{1,0:T(8,128)(2,1)} %tokens_ref.1, bf16[96,1024]{1,0:T(8,128)(2,1)} %grads_ref.1, bf16[3,352,256]{2,1,0:T(8,128)(2,1)} %pad_maximum_fusion.w_ref), custom_call_target="tpu_custom_call" | custom-call | tf_op jit(solution)/shard_map/pallas_call | solution.py:309
  98.8 0.0 copy-start.1
  98.8 3.2 %bitcast_convert_fusion.1 = (f32[256,1408]{1,0:T(8,128)}, f32[256,1408]{1,0:T(8,128)}) fusion(bf16[2,256,1408]{2,1,0:T(8,128)(2,1)} %get-tuple-element.8), kind=kLoop, calls=%fused_computation.1 | loop fusion | flops 720896 | bytes 4325376 | tf_op jit(solution)/shard_map/convert_element_type | solution.py:340
  102.0 0.0 copy-start.2
  102.0 0.0 copy-done.1
  102.0 1.3 %bitcast_convert_fusion = f32[1408,256]{1,0:T(8,128)} fusion(bf16[4,352,256]{2,1,0:T(8,128)(2,1)S(1)} %copy-done.1), kind=kLoop, calls=%fused_computation | loop fusion | flops 360448 | bytes 2162688 | tf_op jit(solution)/shard_map/convert_element_type | solution.py:341
  103.2 0.0 copy-done.2
  103.2 0.7 copy.14
  (1 shorter events, 0.0 us)
Async XLA Ops:
  0.6 1.6 %copy-start = (bf16[1408,256]{1,0:T(8,128)(2,1)S(1)}, bf16[1408,256]{1,0:T(8,128)(2,1)}, u32[]{:S(2)}) copy-start(bf16[1408,256]{1,0:T(8,128)(2,1)} %param.9) | copy-start | bytes 2162692
  98.8 3.2 %copy-start.1 = (bf16[4,352,256]{2,1,0:T(8,128)(2,1)S(1)}, bf16[4,352,256]{2,1,0:T(8,128)(2,1)}, u32[]{:S(2)}) copy-start(bf16[4,352,256]{2,1,0:T(8,128)(2,1)} %get-tuple-element.9) | copy-start | bytes 2162692
  102.0 1.3 %copy-start.2 = (bf16[96,1024]{1,0:T(8,128)(2,1)S(1)}, bf16[96,1024]{1,0:T(8,128)(2,1)}, u32[]{:S(2)}) copy-start(bf16[96,1024]{1,0:T(8,128)(2,1)} %get-tuple-element.18) | copy-start | bytes 589828
